TPU v7x, 32 devices: a whole 2x2x4 slice. The times are simulated.
32 devices in a mesh: sp: 4 (over z), fs: 4 (over y, x), tp: 2 (over core).
Axes of the slice: x: 2, y: 2, z: 4, core: 2. Of those that a mesh axis runs over, the one named last changes fastest.
Arguments:
- tokens: bfloat16 [8192, 2048], P(('fs', 'sp')), parts along dimension 0, may hold values from -6 to 6
- norm_gain: bfloat16 [2048], replicated, may hold values from 0.099609375 to 1.8984375
- w_query: bfloat16 [2048, 1024], P('sp', 'tp'), may hold values from -0.15625 to 0.15625
- w_key: bfloat16 [2048, 256], P('sp', 'tp'), may hold values from -0.15625 to 0.15625
- w_value: bfloat16 [2048, 256], P('sp', 'tp'), may hold values from -0.125 to 0.125
- w_glu_value: bfloat16 [2048, 1024], P('sp', 'tp'), may hold values from -0.22097087 to 0.22097087
- w_glu_gate: bfloat16 [2048, 1024], P('sp', 'tp'), may hold values from -0.125 to 0.125
- conv_taps: bfloat16 [31, 1024], P(None, 'tp'), may hold values from -1 to 1
- convolution_norm_gain: bfloat16 [1024], replicated, may hold values from 0.099609375 to 1.8984375
- head_gain: bfloat16 [128], replicated, may hold values from 0.099609375 to 1.8984375
- lam: float32 [8], P('tp'), may hold values from 0.3 to 0.8
- w_out: bfloat16 [2048, 2048], P(None, 'sp'), may hold values from -0.125 to 0.125
Outputs:
- mixed: bfloat16 [8192, 2048], P(('fs', 'sp', 'tp')), parts along dimension 0
- log_totals: float32 [8192, 16], P(('fs', 'sp'), 'tp'), parts along dimension 0
There are 4 independent parts, one for each index of `fs`. A program takes and returns all parts, laid end to end along the dimension named above; an argument that names none is the same for every part. Nothing has to cross between parts.
All inputs are finite; a program needn't handle non-finite values.
Results may differ from a plain program's by a relative error of at most 0.0095.
Values may be sent and summed in bfloat16 or wider, within the bound.
A program may use at most 64 MiB of HBM per device.

v0:
```python
import math

import jax
import jax.numpy as jnp
from jax import lax
from jax.sharding import PartitionSpec as P

HEADS = 8
QK = 64
VDIM = 128
CONV = 1024


def from_behind(array, axis, by):
    peers = lax.axis_size(axis)
    pairs = [(i, i + by) for i in range(peers) if 0 <= i + by < peers]
    return lax.ppermute(array, axis, pairs)


def body(
    tokens,
    norm_gain,
    w_query,
    w_key,
    w_value,
    w_glu_value,
    w_glu_gate,
    conv_taps,
    convolution_norm_gain,
    head_gain,
    lam,
    w_out,
):
    rows = tokens.shape[0]
    eps = 1e-06
    tok32 = tokens.astype(jnp.float32)
    normalized_rows = (
        tok32
        * lax.rsqrt(jnp.mean(tok32 * tok32, axis=-1, keepdims=True) + eps)
        * norm_gain.astype(jnp.float32)
    ).astype(jnp.bfloat16)
    weights = (w_query, w_key, w_value, w_glu_value, w_glu_gate)
    pieces = (
        lax.all_gather(weights[0], "sp", axis=0, tiled=True),
        lax.all_gather(weights[1], "sp", axis=0, tiled=True),
        lax.all_gather(weights[2], "sp", axis=0, tiled=True),
        lax.all_gather(weights[3], "sp", axis=0, tiled=True),
        lax.all_gather(weights[4], "sp", axis=0, tiled=True),
    )
    proj = tuple(
        (jnp.dot(normalized_rows, piece, preferred_element_type=jnp.float32) for piece in pieces)
    )
    queries = proj[0].astype(jnp.bfloat16)
    keys = proj[1].astype(jnp.bfloat16)
    values = proj[2].astype(jnp.bfloat16)
    gated = (proj[3] * jax.nn.sigmoid(proj[4])).astype(jnp.bfloat16)
    taps = conv_taps.shape[0]
    rim = from_behind(gated[rows - (taps - 1) :], "sp", 1)
    padded = jnp.concatenate([rim, gated], axis=0)
    conv = jnp.zeros(gated.shape, jnp.float32)
    for tap in range(taps):
        conv = conv + conv_taps[tap].astype(jnp.float32) * padded[tap : tap + rows].astype(
            jnp.float32
        )
    conv_out = conv.astype(jnp.bfloat16)
    heads_here = lam.shape[0]
    kv_here = w_key.shape[1] // (2 * QK)
    group = heads_here // kv_here
    query_view = queries.reshape(rows, kv_here, group, 2, QK)
    query_pos = lax.axis_index("sp") * rows + jnp.arange(rows, dtype=jnp.int32)
    scale = QK ** (-0.5)
    empty = (
        jnp.zeros((rows, kv_here, group, 2, VDIM), jnp.float32),
        jnp.zeros((rows, kv_here, group, 2), jnp.float32),
    )
    key_piece = lax.all_gather(keys, "sp", axis=0, tiled=True)
    value_piece = lax.all_gather(values, "sp", axis=0, tiled=True)
    count = key_piece.shape[0]
    width = math.gcd(count, 512)
    blocks = count // width
    key_blocks = key_piece.reshape(blocks, width, kv_here, 2, QK)
    value_blocks = value_piece.reshape(blocks, width, kv_here, VDIM)

    def step(state, item):
        key_block, value_block, index = item
        score = (
            jnp.einsum(
                "tkgmd,nkmd->tkgmn", query_view, key_block, preferred_element_type=jnp.float32
            )
            * scale
        )
        key_pos = index * width + jnp.arange(width, dtype=jnp.int32)
        allowed = key_pos[None, None, None, None, :] <= query_pos[:, None, None, None, None]
        weight = jnp.where(allowed, jnp.exp(score), 0.0)
        running_total = state[0] + jnp.einsum(
            "doejz,zow->doejw",
            weight.astype(jnp.bfloat16),
            value_block,
            preferred_element_type=jnp.float32,
        )
        total = state[1] + jnp.sum(weight, axis=-1)
        return ((running_total, total), None)

    result, _ = lax.scan(
        step, empty, (key_blocks, value_blocks, jnp.arange(blocks, dtype=jnp.int32))
    )
    running_total, total = result
    running_total = running_total.reshape(rows, heads_here, 2, VDIM)
    total = total.reshape(rows, heads_here, 2)
    diff = (
        running_total[:, :, 0] / total[:, :, 0, None]
        - lam[None, :, None] * running_total[:, :, 1] / total[:, :, 1, None]
    )
    att_out = (
        diff
        * lax.rsqrt(jnp.mean(diff * diff, axis=-1, keepdims=True) + eps)
        * head_gain.astype(jnp.float32)
    )
    att_out = att_out.astype(jnp.bfloat16).reshape(rows, heads_here * VDIM)
    log_totals = jnp.log(total).reshape(rows, heads_here * 2)
    pair_index = lax.axis_index("tp")
    channels_here = conv_out.shape[1]
    att_rows_here = att_out.shape[1]
    conv32 = conv_out.astype(jnp.float32)
    squares = lax.psum(jnp.sum(conv32 * conv32, axis=-1), "tp")
    gain_here = lax.dynamic_slice_in_dim(
        convolution_norm_gain, pair_index * channels_here, channels_here, 0
    ).astype(jnp.float32)
    conv_act = jax.nn.silu(conv32 * lax.rsqrt(squares / CONV + eps)[:, None] * gain_here).astype(
        jnp.bfloat16
    )
    both = jnp.concatenate([att_out, conv_act], axis=1)
    att_weight = lax.dynamic_slice_in_dim(w_out, pair_index * att_rows_here, att_rows_here, 0)
    conv_weight = lax.dynamic_slice_in_dim(
        w_out, HEADS * VDIM + pair_index * channels_here, channels_here, 0
    )
    weight_here = jnp.concatenate([att_weight, conv_weight], axis=0)
    weight_full = lax.all_gather(weight_here, "sp", axis=1, tiled=True)
    mixed = lax.psum_scatter(
        jnp.dot(both, weight_full, preferred_element_type=jnp.float32).astype(jnp.bfloat16),
        "tp",
        scatter_dimension=0,
        tiled=True,
    )
    return (mixed, log_totals)


def solution(mesh):
    return jax.shard_map(
        body,
        mesh=mesh,
        in_specs=(
            P(("fs", "sp"), None),
            P(),
            P("sp", "tp"),
            P("sp", "tp"),
            P("sp", "tp"),
            P("sp", "tp"),
            P("sp", "tp"),
            P(None, "tp"),
            P(),
            P(),
            P("tp"),
            P(None, "sp"),
        ),
        out_specs=(P(("fs", "sp", "tp"), None), P(("fs", "sp"), "tp")),
        check_vma=False,
    )
```

profile of v0, /device:TPU:25, one launch (start us, length us, event | category | flops | bytes accessed | tf_op | source)
XLA Modules:
  0.0 276.9 jit_solution(3802252638703074889)
XLA Ops:
  14.8 21.4 %all_gather.26 = bf16[2048,128]{1,0:T(8,128)(2,1)S(1)} all-gather(bf16[512,128]{1,0:T(8,128)(2,1)S(1)} %copy-done.3), channel_id=1, replica_groups=mesh['sp'=4,'fs'=4,'tp'=2] {'sp'}, dimensions={0}, use_global_device_ids=true | all-gather | bytes 655360 | tf_op jit(solution)/shard_map/all_gather | solution.py:45
  37.0 21.5 %all_gather.27 = bf16[2048,128]{1,0:T(8,128)(2,1)} all-gather(bf16[512,128]{1,0:T(8,128)(2,1)S(1)} %convolution_convert_fusion.2), channel_id=1, replica_groups=mesh['sp'=4,'fs'=4,'tp'=2] {'sp'}, dimensions={0}, use_global_device_ids=true | all-gather | bytes 655360 | tf_op jit(solution)/shard_map/all_gather | solution.py:76
  58.5 2.4 reshape.150
  62.8 15.2 %all_gather.24 = bf16[2048,128]{1,0:T(8,128)(2,1)S(1)} all-gather(bf16[512,128]{1,0:T(8,128)(2,1)S(1)} %copy-done.4), channel_id=1, replica_groups=mesh['sp'=4,'fs'=4,'tp'=2] {'sp'}, dimensions={0}, use_global_device_ids=true | all-gather | bytes 655360 | tf_op jit(solution)/shard_map/all_gather | solution.py:46
  80.5 20.7 %all_gather.25 = bf16[2048,128]{1,0:T(8,128)(2,1)S(1)} all-gather(bf16[512,128]{1,0:T(8,128)(2,1)S(1)} %convolution_convert_fusion.3), channel_id=1, replica_groups=mesh['sp'=4,'fs'=4,'tp'=2] {'sp'}, dimensions={0}, use_global_device_ids=true | all-gather | bytes 655360 | tf_op jit(solution)/shard_map/all_gather | solution.py:77
  101.9 3.6 %convolution_convert_fusion.1 = bf16[512,512]{0,1:T(8,128)(2,1)S(1)} fusion(bf16[2048,512]{1,0:T(8,128)(2,1)} %all-gather.5.cloned.1.call-done, bf16[512,2048]{1,0:T(8,128)(2,1)} %param.14, f32[2048]{0:T(1024)} %copy-done.10, f32[512]{0:T(512)} %copy-done.14), kind=kOutput, calls=%fused_computation.62 | convolution fusion | flops 1078198272 | bytes 4728832 | tf_op jit(solution)/shard_map/dot_general | solution.py:51
  105.6 39.8 %while.13 = (s32[]{:T(128)}, f32[512,1,4,2,128]{0,4,3,2,1:T(8,128)S(1)}, f32[512,1,4,2]{0,2,3,1:T(4,128)S(1)}, bf16[4,512,1,128]{3,1,0,2:T(8,128)(2,1)S(1)}, s32...) while((s32[]{:T(128)}, ...), condition=%wide.region_3.4_spmd.clone, body=%wide.region_1.3_spmd.clone.sunk | while | flops 815010816 | bytes 13968028 | solution.py:104
  107.0 5.1 %fusion.96 = (f32[512,4,2]{0,1,2:T(4,128)S(1)}, bf16[512,4,2,512]{0,3,1,2:T(8,128)(2,1)}) fusion(pred[512,512]{0,1:T(8,128)(4,1)S(1)} %broadcast_compare_fusion.2, bf16[512,1,4,2,64]{0,4,2,3,1:T(8,128)(2,1)S(1)} %get-tuple-element.247, bf16[4,512,1,2,64]{1,4,3,2,0:T(8,128)(2,1)} %get-tuple-element.246, s32[]{:T(128)} %get-tuple-element.230), kind=kOutput, calls=%fused_computation.2.clone.1 | convolution fusion | flops 276819968 | bytes 5128704 | tf_op jit(solution)/shard_map/while/body/eval_jaxpr/tkgmd,nkmd->tkgmn/dot_general | solution.py:87
  112.2 3.3 %bitcast_add_fusion.4 = f32[512,1,4,2,128]{0,4,3,2,1:T(8,128)S(1)} fusion(f32[512,1,4,2,128]{0,4,3,2,1:T(8,128)S(1)} %get-tuple-element.231, bf16[512,4,2,512]{0,3,1,2:T(8,128)(2,1)} %get-tuple-element.217, pred[]{:T(512)S(6)} %compare.3, bf16[4,512,1,128]{3,1,0,2:T(8,128)(2,1)S(1)} %get-tuple-element.244, s32[]{:T(128)} %get-tuple-element.230), kind=kOutput, calls=%fused_computation.7.clone.1 | convolution fusion | flops 537919488 | bytes 8519685 | tf_op jit(solution)/shard_map/while/body/eval_jaxpr/doejz,zow->doejw/dot_general | solution.py:95
  117.0 5.1 %fusion.96 = (f32[512,4,2]{0,1,2:T(4,128)S(1)}, bf16[512,4,2,512]{0,3,1,2:T(8,128)(2,1)}) fusion(pred[512,512]{0,1:T(8,128)(4,1)S(1)} %broadcast_compare_fusion.2, bf16[512,1,4,2,64]{0,4,2,3,1:T(8,128)(2,1)S(1)} %get-tuple-element.247, bf16[4,512,1,2,64]{1,4,3,2,0:T(8,128)(2,1)} %get-tuple-element.246, s32[]{:T(128)} %get-tuple-element.230), kind=kOutput, calls=%fused_computation.2.clone.1 | convolution fusion | flops 276819968 | bytes 5128704 | tf_op jit(solution)/shard_map/while/body/eval_jaxpr/tkgmd,nkmd->tkgmn/dot_general | solution.py:87
  122.1 3.3 %bitcast_add_fusion.4 = f32[512,1,4,2,128]{0,4,3,2,1:T(8,128)S(1)} fusion(f32[512,1,4,2,128]{0,4,3,2,1:T(8,128)S(1)} %get-tuple-element.231, bf16[512,4,2,512]{0,3,1,2:T(8,128)(2,1)} %get-tuple-element.217, pred[]{:T(512)S(6)} %compare.3, bf16[4,512,1,128]{3,1,0,2:T(8,128)(2,1)S(1)} %get-tuple-element.244, s32[]{:T(128)} %get-tuple-element.230), kind=kOutput, calls=%fused_computation.7.clone.1 | convolution fusion | flops 537919488 | bytes 8519685 | tf_op jit(solution)/shard_map/while/body/eval_jaxpr/doejz,zow->doejw/dot_general | solution.py:95
  126.9 5.1 %fusion.96 = (f32[512,4,2]{0,1,2:T(4,128)S(1)}, bf16[512,4,2,512]{0,3,1,2:T(8,128)(2,1)}) fusion(pred[512,512]{0,1:T(8,128)(4,1)S(1)} %broadcast_compare_fusion.2, bf16[512,1,4,2,64]{0,4,2,3,1:T(8,128)(2,1)S(1)} %get-tuple-element.247, bf16[4,512,1,2,64]{1,4,3,2,0:T(8,128)(2,1)} %get-tuple-element.246, s32[]{:T(128)} %get-tuple-element.230), kind=kOutput, calls=%fused_computation.2.clone.1 | convolution fusion | flops 276819968 | bytes 5128704 | tf_op jit(solution)/shard_map/while/body/eval_jaxpr/tkgmd,nkmd->tkgmn/dot_general | solution.py:87
  132.0 3.3 %bitcast_add_fusion.4 = f32[512,1,4,2,128]{0,4,3,2,1:T(8,128)S(1)} fusion(f32[512,1,4,2,128]{0,4,3,2,1:T(8,128)S(1)} %get-tuple-element.231, bf16[512,4,2,512]{0,3,1,2:T(8,128)(2,1)} %get-tuple-element.217, pred[]{:T(512)S(6)} %compare.3, bf16[4,512,1,128]{3,1,0,2:T(8,128)(2,1)S(1)} %get-tuple-element.244, s32[]{:T(128)} %get-tuple-element.230), kind=kOutput, calls=%fused_computation.7.clone.1 | convolution fusion | flops 537919488 | bytes 8519685 | tf_op jit(solution)/shard_map/while/body/eval_jaxpr/doejz,zow->doejw/dot_general | solution.py:95
  136.8 5.2 %fusion.96 = (f32[512,4,2]{0,1,2:T(4,128)S(1)}, bf16[512,4,2,512]{0,3,1,2:T(8,128)(2,1)}) fusion(pred[512,512]{0,1:T(8,128)(4,1)S(1)} %broadcast_compare_fusion.2, bf16[512,1,4,2,64]{0,4,2,3,1:T(8,128)(2,1)S(1)} %get-tuple-element.247, bf16[4,512,1,2,64]{1,4,3,2,0:T(8,128)(2,1)} %get-tuple-element.246, s32[]{:T(128)} %get-tuple-element.230), kind=kOutput, calls=%fused_computation.2.clone.1 | convolution fusion | flops 276819968 | bytes 5128704 | tf_op jit(solution)/shard_map/while/body/eval_jaxpr/tkgmd,nkmd->tkgmn/dot_general | solution.py:87
  142.0 3.3 %bitcast_add_fusion.4 = f32[512,1,4,2,128]{0,4,3,2,1:T(8,128)S(1)} fusion(f32[512,1,4,2,128]{0,4,3,2,1:T(8,128)S(1)} %get-tuple-element.231, bf16[512,4,2,512]{0,3,1,2:T(8,128)(2,1)} %get-tuple-element.217, pred[]{:T(512)S(6)} %compare.3, bf16[4,512,1,128]{3,1,0,2:T(8,128)(2,1)S(1)} %get-tuple-element.244, s32[]{:T(128)} %get-tuple-element.230), kind=kOutput, calls=%fused_computation.7.clone.1 | convolution fusion | flops 537919488 | bytes 8519685 | tf_op jit(solution)/shard_map/while/body/eval_jaxpr/doejz,zow->doejw/dot_general | solution.py:95
  149.7 2.6 copy.53
  157.1 4.7 %fusion.22 = f32[512,512]{1,0:T(8,128)} fusion(bf16[2048,512]{1,0:T(8,128)(2,1)} %all-gather.9.cloned.1.call-done, bf16[512,2048]{1,0:T(8,128)(2,1)} %param.14, f32[2048]{0:T(1024)S(1)} %copy-done.11, f32[512]{0:T(512)} %copy-done.14), kind=kOutput, calls=%fused_computation.61 | convolution fusion | flops 1078722560 | bytes 5253120 | tf_op jit(solution)/shard_map/dot_general | solution.py:51
  161.7 10.3 %all-gather.7.cloned.1.call-done = bf16[2048,512]{1,0:T(8,128)(2,1)} async-done(((bf16[512,512]{1,0:T(8,128)(2,1)}), bf16[2048,512]{1,0:T(8,128)(2,1)}) %all-gather.7.cloned.1.call-update) | async-done | bytes 2097168 | tf_op jit(solution)/shard_map/all_gather | solution.py:47
  172.0 3.8 %fusion.23 = bf16[512,512]{1,0:T(8,128)(2,1)S(1)} fusion(f32[512,512]{1,0:T(8,128)} %fusion.22, bf16[2048,512]{1,0:T(8,128)(2,1)} %all-gather.7.cloned.1.call-done, bf16[512,2048]{1,0:T(8,128)(2,1)} %param.14, f32[2048]{0:T(1024)S(1)} %copy-done.11, f32[512]{0:T(512)} %copy-done.14), kind=kOutput, calls=%fused_computation.63 | convolution fusion | flops 1078460416 | bytes 5777408 | tf_op jit(solution)/shard_map/dot_general | solution.py:51
  180.7 4.7 %fusion.24 = (f32[512]{0:T(512)S(1)}, bf16[512,512]{1,0:T(8,128)(2,1)S(1)}) fusion(bf16[512,512]{1,0:T(8,128)(2,1)S(1)} %fusion.23, f32[512]{0:T(512)S(1)} %bitcast.175, bf16[30,512]{1,0:T(8,128)(2,1)S(1)} %collective-permute-done, f32[512]{0:T(512)S(1)} %bitcast.176, f32[512]{0:T(512)S(1)} %bitcast.147, f32[512]{0:T(512)S(1)} %bitcast.148, ...), kind=kLoop, calls=%fused_computation.66 | loop fusion | flops 48758272 | bytes 1144832 | tf_op jit(solution)/shard_map/reduce_sum | solution.py:125
  185.4 3.8 %psum.7 = f32[512]{0:T(512)S(1)} all-reduce(f32[512]{0:T(512)S(1)} %get-tuple-element.117), channel_id=1, replica_groups=mesh['sp'=4,'fs'=4,'tp'=2] {'tp'}, use_global_device_ids=true, to_apply=%region_6.7 | all-reduce | flops 512 | bytes 4096 | tf_op jit(solution)/shard_map/psum | solution.py:125
  189.5 63.3 %all-gather.11.cloned.1.call-done = bf16[1024,2048]{1,0:T(8,128)(2,1)} async-done(((bf16[1024,512]{1,0:T(8,128)(2,1)}), bf16[1024,2048]{1,0:T(8,128)(2,1)}) %all-gather.11.cloned.1.call-update) | async-done | bytes 4194320 | tf_op jit(solution)/shard_map/all_gather | solution.py:138
  252.8 5.9 %convolution_convert_fusion = bf16[512,2048]{1,0:T(8,128)(2,1)} fusion(bf16[1024,2048]{1,0:T(8,128)(2,1)} %all-gather.11.cloned.1.call-done, bf16[512,512]{1,0:T(8,128)(2,1)S(1)} %fusion.31, bf16[512,512]{1,0:T(8,128)(2,1)S(1)} %copy-done.2), kind=kOutput, calls=%fused_computation.54 | convolution fusion | flops 2150629376 | bytes 7340032 | tf_op jit(solution)/shard_map/dot_general | solution.py:140
  259.4 11.0 %reduce-scatter.2.cloned.1.call-done = bf16[256,2048]{1,0:T(8,128)(2,1)} async-done(((bf16[512,2048]{1,0:T(8,128)(2,1)}), bf16[256,2048]{1,0:T(8,128)(2,1)}) %reduce-scatter.2.cloned.1.call-update) | async-done | bytes 1048592 | tf_op jit(solution)/shard_map/reduce_scatter | solution.py:139
  (99 shorter events, 31.5 us)
Async XLA Ops:
  7.2 94.7 %all-gather.5.cloned.1.call-start = ((), (), s32[]{:S(2)}) async-start(), calls=%async_computation.1 | async-start | bytes 2621440 | tf_op jit(solution)/shard_map/all_gather | solution.py:44
  7.9 149.1 %all-gather.9.cloned.1.call-start = ((), (), s32[]{:S(2)}) async-start(), calls=%async_computation.3 | async-start | bytes 2621440 | tf_op jit(solution)/shard_map/all_gather | solution.py:48
  8.6 163.4 %all-gather.7.cloned.1.call-start = ((), (), s32[]{:S(2)}) async-start(), calls=%async_computation.2 | async-start | bytes 2621440 | tf_op jit(solution)/shard_map/all_gather | solution.py:47
  9.4 243.4 %all-gather.11.cloned.1.call-start = ((), (), s32[]{:S(2)}) async-start(), calls=%async_computation.4 | async-start | bytes 5242880 | tf_op jit(solution)/shard_map/all_gather | solution.py:138
  10.7 1.2 copy-start.5
  10.7 1.8 copy-start.12
  11.8 3.0 %copy-start.3 = (bf16[512,128]{1,0:T(8,128)(2,1)S(1)}, bf16[512,128]{1,0:T(8,128)(2,1)}, u32[]{:S(2)}) copy-start(bf16[512,128]{1,0:T(8,128)(2,1)} %param.17) | copy-start | bytes 393220
  11.8 258.6 %reduce-scatter.2.cloned.1.call-start = ((), (), s32[]{:S(2)}) async-start(), calls=%async_computation.5 | async-start | bytes 3145728 | tf_op jit(solution)/shard_map/reduce_scatter | solution.py:139
  12.5 23.7 %copy-start.1 = (bf16[512,2048]{1,0:T(8,128)(2,1)S(1)}, bf16[512,2048]{1,0:T(8,128)(2,1)}, u32[]{:S(2)}) copy-start(bf16[512,2048]{1,0:T(8,128)(2,1)} %param.14) | copy-start | bytes 6291460
  12.5 65.5 %copy-start.10 = (f32[2048]{0:T(1024)}, f32[2048]{0:T(1024)S(1)}, u32[]{:S(2)}) copy-start(f32[2048]{0:T(1024)S(1)} %convert_element_type.202) | copy-start | bytes 24580
  14.8 63.3 %copy-start.14 = (f32[512]{0:T(512)}, f32[512]{0:T(512)S(1)}, u32[]{:S(2)}) copy-start(f32[512]{0:T(512)S(1)} %add_rsqrt_fusion.2) | copy-start | bytes 6148
  37.0 25.8 %copy-start.4 = (bf16[512,128]{1,0:T(8,128)(2,1)S(1)}, bf16[512,128]{1,0:T(8,128)(2,1)}, u32[]{:S(2)}) copy-start(bf16[512,128]{1,0:T(8,128)(2,1)} %param.18) | copy-start | bytes 393220
  78.0 23.2 %copy-start.16 = (bf16[128]{0:T(256)(128)(2,1)S(1)}, bf16[128]{0:T(256)(128)(2,1)}, u32[]{:S(2)}) copy-start(bf16[128]{0:T(256)(128)(2,1)} %param.23) | copy-start | bytes 772
  78.0 23.2 %copy-start.13 = (f32[4]{0:T(128)S(1)}, f32[4]{0:T(128)}, u32[]{:S(2)}) copy-start(f32[4]{0:T(128)} %param.24) | copy-start | bytes 52
  78.0 23.2 %copy-start.15 = (bf16[1024]{0:T(1024)(128)(2,1)S(1)}, bf16[1024]{0:T(1024)(128)(2,1)}, u32[]{:S(2)}) copy-start(bf16[1024]{0:T(1024)(128)(2,1)} %param.22) | copy-start | bytes 6148
  153.9 3.2 %copy-start.11 = (f32[2048]{0:T(1024)S(1)}, f32[2048]{0:T(1024)}, u32[]{:S(2)}) copy-start(f32[2048]{0:T(1024)} %copy-done.10) | copy-start | bytes 24580
  175.8 2.1 copy-start
  175.9 4.8 %collective-permute-start = (bf16[30,512]{1,0:T(8,128)(2,1)S(1)}, bf16[30,512]{1,0:T(8,128)(2,1)S(1)}, u32[]{:S(2)}, u32[]{:S(2)}) collective-permute-start(bf16[30,512]{1,0:T(8,128)(2,1)S(1)} %slice.268), channel_id=1, source_target_pairs={{0,8},{8,16},{16,24},{1,9},{9,17},{17,25},{2,10},{10,18},{18,26},{... | collective-permute-start | bytes 92168 | tf_op jit(solution)/shard_map/ppermute | solution.py:17
  177.9 2.8 copy-start.6
  177.9 2.7 copy-start.7
  177.9 2.7 copy-start.8
  177.9 11.2 %copy-start.9 = (f32[512]{0:T(512)S(1)}, f32[512]{0:T(512)}, u32[]{:S(2)}) copy-start(f32[512]{0:T(512)} %dynamic-slice_convert_fusion) | copy-start | bytes 6148
  179.4 73.4 %copy-start.2 = (bf16[512,512]{1,0:T(8,128)(2,1)S(1)}, bf16[512,512]{1,0:T(8,128)(2,1)}, u32[]{:S(2)}) copy-start(bf16[512,512]{1,0:T(8,128)(2,1)} %fusion.33) | copy-start | bytes 1572868
Sparse Core Ops, SparseCore 0:
  9.5 61.2 all-gather.4
  72.4 53.3 all-gather.8
  127.3 44.6 all-gather.6
  174.0 78.7 all-gather.10
  258.8 11.5 reduce-scatter.1
where the time goes:
time: 279 us; the launch traced here: 277 us
  waiting for transfers between devices  88 us (32%)
  blocking collectives  82.6 us (30%)
  matrix products  54.9 us (20%)
  local copies, waits for them, and re-layouts  20.7 us (7%)
  between operations  14.1 us (5%)
  other arithmetic  12.3 us (4%)
    all_gather x1, waiting for transfers between devices, body(): weight_full = lax.all_gather(weight_here, 'sp', axis=1, tiled=True)  63.3 us
    all_gather x1, blocking collectives, body(): key_piece = lax.all_gather(keys, 'sp', axis=0, tiled=True)  21.5 us
    all_gather x1, blocking collectives, body(): lax.all_gather(weights[1], 'sp', axis=0, tiled=True)  21.4 us
    all_gather x1, blocking collectives, body(): value_piece = lax.all_gather(values, 'sp', axis=0, tiled=True)  20.7 us
    dot_general x4, matrix products, step(): jnp.einsum('tkgmd,nkmd->tkgmn', query_view, key_block, preferred_element_...  20.5 us
    dot_general x5, matrix products, body(): jnp.dot(normalized_rows, piece, preferred_element_type=jnp.float32)  15.3 us
    all_gather x1, blocking collectives, body(): lax.all_gather(weights[2], 'sp', axis=0, tiled=True)  15.2 us
    dot_general x4, matrix products, step(): jnp.einsum('doejz,zow->doejw', weight.astype(jnp.bfloat16), value_block,...  13.2 us
  transfers between devices with their start and end apart: 6, of which 4 were waited for; matrix products, arithmetic and copies ran while one was open for 30% of the time, Pallas kernels for 0%

commit v1 on v0

v1 whole, which is shorter than its diff:
```python
import functools
import math

import jax
import jax.numpy as jnp
from jax import lax
from jax.experimental import pallas as pl
from jax.experimental.pallas import tpu as pltpu
from jax.sharding import PartitionSpec as P

QK = 64
VDIM = 128
EPS = 1e-06
MESH = pl.DeviceIdType.MESH
BF = jnp.bfloat16
F32 = jnp.float32
LANES = 128
RIM = 32


def kernel(
    n,
    conv_total,
    tok_h,
    gain_r,
    wq_h,
    wk_h,
    wv_h,
    wgv_h,
    wgg_h,
    taps_r,
    cgain_r,
    hgain_r,
    lam_r,
    wo_h,
    mixed_r,
    log_r,
    tok,
    normed,
    ga,
    gb,
    gc,
    q2,
    kbuf,
    vbuf,
    acc,
    gated,
    rim,
    pad,
    conv,
    sq_own,
    sq_in,
    both,
    part_out,
    part_in,
    keep,
    loc,
    zs,
    zr,
    xs,
    xr,
    ys,
    yr,
    hxs,
    hxr,
    hys,
    hyr,
    kvs,
    kvr,
    rims,
    sqs,
    ps,
    pr,
):
    s = lax.axis_index("sp")
    f = lax.axis_index("fs")
    t = lax.axis_index("tp")
    fx = f + 1 - 2 * (f % 2)
    fy = (f + 2) % 4
    left = {"sp": s - 1, "fs": f, "tp": t}
    right = {"sp": s + 1, "fs": f, "tp": t}
    xdev = {"sp": s, "fs": fx, "tp": t}
    ydev = {"sp": s, "fs": fy, "tp": t}
    mate = {"sp": s, "fs": f, "tp": 1 - t}
    rows, width = tok.shape
    heads = lam_r.shape[0]
    chans = gated.shape[1]
    qcols = wq_h.shape[1]
    half = rows // 2
    groups = (ga, gb, gc)
    has_left = s > 0
    has_right = s < n - 1

    d_rows = wq_h.shape[0]
    att_rows = heads * VDIM
    locals_ = [
        (wq_h, ga.at[s, :, pl.ds(0, qcols)]),
        (wk_h, ga.at[s, :, pl.ds(qcols, LANES)]),
        (wv_h, ga.at[s, :, pl.ds(qcols + LANES, LANES)]),
        (tok_h, tok),
        (wgv_h, gb.at[s, :, pl.ds(0, chans)]),
        (wgg_h, gb.at[s, :, pl.ds(chans, chans)]),
        (wo_h.at[pl.ds(t * att_rows, att_rows), :], gc.at[s, pl.ds(0, att_rows), :]),
        (
            wo_h.at[pl.ds(2 * att_rows + t * chans, chans), :],
            gc.at[s, pl.ds(att_rows, chans), :],
        ),
    ]
    copies = [pltpu.make_async_copy(a, b, loc.at[i]) for i, (a, b) in enumerate(locals_)]
    for c in copies:
        c.start()

    bar = pltpu.get_barrier_semaphore()
    for dev in (xdev, ydev, mate):
        pl.semaphore_signal(bar, 1, device_id=dev, device_id_type=MESH)

    @pl.when(has_left)
    def _():
        pl.semaphore_signal(bar, 1, device_id=left, device_id_type=MESH)

    @pl.when(has_right)
    def _():
        pl.semaphore_signal(bar, 1, device_id=right, device_id_type=MESH)

    pl.semaphore_wait(bar, 3 + jnp.where(has_left, 1, 0) + jnp.where(has_right, 1, 0))

    def chunk(g, o, q, part=None):
        buf = groups[g]
        size = buf.shape[1] // 4
        if part is None:
            return buf.at[o, pl.ds(pl.multiple_of(q * size, size), size), :]
        size = size // 2
        return buf.at[o, pl.ds(pl.multiple_of((q * 2 + part) * size, size), size), :]

    def zcopy(g, o, right_way):
        c = chunk(g, o, f)
        return pltpu.make_async_remote_copy(
            c,
            c,
            zs.at[g, 0 if right_way else 1, o],
            zr.at[g, o],
            device_id=right if right_way else left,
            device_id_type=MESH,
        )

    def xcopy(g, o, q):
        c = chunk(g, o, q)
        return pltpu.make_async_remote_copy(
            c, c, xs.at[g, o], xr.at[g, o], device_id=xdev, device_id_type=MESH
        )

    def ycopy(g, o, q):
        c = chunk(g, o, q)
        return pltpu.make_async_remote_copy(
            c, c, ys.at[g, o], yr.at[g, o], device_id=ydev, device_id_type=MESH
        )

    def hxcopy(g, o, q):
        c = chunk(g, o, q, 0)
        return pltpu.make_async_remote_copy(
            c, c, hxs.at[g, o], hxr.at[g, o], device_id=xdev, device_id_type=MESH
        )

    def hycopy(g, o, q):
        c = chunk(g, o, q, 1)
        return pltpu.make_async_remote_copy(
            c, c, hys.at[g, o], hyr.at[g, o], device_id=ydev, device_id_type=MESH
        )

    fd = 3 - f

    def sides(k, fn):
        @pl.when(s >= k)
        def _():
            fn(s - k, True)

        @pl.when(s + k < n)
        def _():
            fn(s + k, False)

    def own_send(g):
        @pl.when(has_right)
        def _():
            zcopy(g, s, True).start()

        @pl.when(has_left)
        def _():
            zcopy(g, s, False).start()

    def stage1(g, k):
        def go(o, right_way):
            zcopy(g, o, right_way).wait_recv()
            xcopy(g, o, f).start()
            ycopy(g, o, f).start()

            @pl.when(has_right if right_way else has_left)
            def _():
                zcopy(g, o, right_way).start()

        sides(k, go)

    def stage2(g, k):
        def go(o, right_way):
            xcopy(g, o, fx).wait_recv()
            hycopy(g, o, fx).start()
            ycopy(g, o, fy).wait_recv()
            hxcopy(g, o, fy).start()

        sides(k, go)

    def stage3(g, k):
        def go(o, right_way):
            hxcopy(g, o, fd).wait_recv()
            hycopy(g, o, fd).wait_recv()

        sides(k, go)

    def drain(g):
        own = zcopy(g, s, True)

        @pl.when(has_right)
        def _():
            own.wait_send()

        @pl.when(has_left)
        def _():
            zcopy(g, s, False).wait_send()

        for k in range(1, n):

            def go(o, right_way):
                xcopy(g, o, f).wait_send()
                ycopy(g, o, f).wait_send()
                hycopy(g, o, fx).wait_send()
                hxcopy(g, o, fy).wait_send()

                @pl.when(has_right if right_way else has_left)
                def _():
                    zcopy(g, o, right_way).wait_send()

            sides(k, go)

    def kvcopy(o):
        return [
            pltpu.make_async_remote_copy(
                b.at[o], b.at[o], kvs.at[i, o], kvr.at[i, o], device_id=right, device_id_type=MESH
            )
            for i, b in enumerate((kbuf, vbuf))
        ]

    def kv_take(k):
        @pl.when(s >= k)
        def _():
            for c in kvcopy(s - k):
                c.wait_recv()

            @pl.when(has_right)
            def _():
                for c in kvcopy(s - k):
                    c.start()

    tall = min(256, rows)
    per_head = 2 * rows // tall

    def attend(o, diagonal):
        vx = jnp.concatenate([vbuf[o], jnp.ones((rows, VDIM), BF)], axis=1)
        kx = kbuf[o]

        def step(i, carry):
            h = i // per_head
            at = pl.multiple_of((i % per_head) * tall, tall)
            score = lax.dot_general(
                q2[h, pl.ds(at, tall), :],
                kx,
                (((1,), (1,)), ((), ())),
                preferred_element_type=F32,
            )
            w = jnp.exp2(score * (QK**-0.5 * math.log2(math.e)))
            if diagonal:
                pos = (at % rows) + lax.broadcasted_iota(jnp.int32, w.shape, 0)
                w = jnp.where(lax.broadcasted_iota(jnp.int32, w.shape, 1) <= pos, w, 0.0)
            pv = jnp.dot(w.astype(BF), vx, preferred_element_type=F32)
            if diagonal:
                acc[h, pl.ds(at, tall), :] = pv
            else:
                acc[h, pl.ds(at, tall), :] += pv
            return carry

        lax.fori_loop(0, heads * per_head, step, 0, unroll=2)

    def attend_back(k):
        @pl.when(s >= k)
        def _():
            attend(s - k, False)

    for c in copies[:3]:
        c.wait()
    own_send(0)
    copies[3].wait()

    def norm_step(i, carry):
        at = pl.ds(pl.multiple_of(i * 32, 32), 32)
        x = tok[at, :].astype(F32)
        r = lax.rsqrt(jnp.mean(x * x, axis=-1, keepdims=True) + EPS)
        normed[at, :] = (x * r * gain_r[...].astype(F32)).astype(BF)
        return carry

    lax.fori_loop(0, rows // 32, norm_step, 0)
    for c in copies[4:]:
        c.wait()

    for k in range(1, n):
        stage1(0, k)
        if k == 1:
            own_send(1)
        if k > 1:
            stage2(0, k - 1)
    if n > 1:
        stage2(0, n - 1)
        stage1(1, 1)
        own_send(2)
    for k in range(1, n):
        stage3(0, k)

    lane = lax.broadcasted_iota(jnp.int32, (rows, LANES), 1)

    kv = jnp.dot(
        normed[...],
        ga[:, :, qcols : qcols + 2 * LANES].reshape(width, 2 * LANES),
        preferred_element_type=F32,
    ).astype(BF)
    kbuf[s] = kv[:, :LANES]
    vbuf[s] = kv[:, LANES:]

    @pl.when(has_right)
    def _():
        for c in kvcopy(s):
            c.start()

    def q_step(h, carry):
        cols = pl.ds(pl.multiple_of(h * 2 * LANES, 2 * LANES), 2 * LANES)
        q = jnp.dot(normed[...], ga[:, :, cols].reshape(width, 2 * LANES), preferred_element_type=F32)
        for e in range(2):
            one = q[:, e * LANES : (e + 1) * LANES]
            q2[2 * h + e, :rows, :] = jnp.where(lane < QK, one, 0.0).astype(BF)
            q2[2 * h + e, rows:, :] = jnp.where(lane >= QK, one, 0.0).astype(BF)
        return carry

    lax.fori_loop(0, heads // 2, q_step, 0)

    if n > 2:
        stage1(1, 2)
    if n > 1:
        stage2(1, 1)
    attend(s, True)
    for k in range(3, n):
        stage1(1, k)
        stage2(1, k - 1)
    if n > 1:
        kv_take(1)
    if n > 2:
        stage2(1, n - 1)
    if n > 1:
        attend_back(1)
        stage1(2, 1)
    for k in range(1, n):
        stage3(1, k)

    def glu_step(i, carry):
        at = pl.multiple_of(i * 2 * LANES, 2 * LANES)
        cols = pl.ds(at, 2 * LANES)
        cols_gate = pl.ds(pl.multiple_of(chans + at, 2 * LANES), 2 * LANES)
        val = jnp.dot(normed[...], gb[:, :, cols].reshape(width, 2 * LANES), preferred_element_type=F32)
        gate = jnp.dot(
            normed[...], gb[:, :, cols_gate].reshape(width, 2 * LANES), preferred_element_type=F32
        )
        g = (val * jax.nn.sigmoid(gate)).astype(BF)
        gated[:, cols] = g
        pad[RIM:, cols] = g.astype(F32)
        return carry

    lax.fori_loop(0, chans // (2 * LANES), glu_step, 0)

    rim_copy = pltpu.make_async_remote_copy(
        gated.at[pl.ds(rows - RIM, RIM), :],
        rim,
        rims.at[0],
        rims.at[1],
        device_id=right,
        device_id_type=MESH,
    )

    @pl.when(has_right)
    def _():
        rim_copy.start()

    for k in range(2, n):
        stage1(2, k)
        stage2(2, k - 1)
        kv_take(k)
        attend_back(k)
    if n > 1:
        stage2(2, n - 1)

    @pl.when(has_left)
    def _():
        rim_copy.wait_recv()
        pad[:RIM, :] = rim[...].astype(F32)

    @pl.when(s == 0)
    def _():
        pad[:RIM, :] = jnp.zeros((RIM, chans), F32)

    taps = taps_r.shape[0]
    shift = RIM - (taps - 1)
    tile = min(128, rows)

    def conv_step(i, carry):
        cols = pl.ds(pl.multiple_of(i * LANES, LANES), LANES)
        for r in range(0, rows, tile):
            total = jnp.zeros((tile, LANES), F32)
            for j in range(taps):
                total = total + taps_r[j : j + 1, cols].astype(F32) * pad[
                    r + shift + j : r + shift + j + tile, cols
                ]
            conv[r : r + tile, cols] = total.astype(BF).astype(F32)
        return carry

    lax.fori_loop(0, chans // LANES, conv_step, 0)
    cv = conv[...]
    sq_own[...] = jnp.broadcast_to(jnp.sum(cv * cv, axis=-1, keepdims=True), (rows, LANES))
    sq_copy = pltpu.make_async_remote_copy(
        sq_own, sq_in, sqs.at[0], sqs.at[1], device_id=mate, device_id_type=MESH
    )
    sq_copy.start()

    def head_rows(i, carry):
        at = pl.multiple_of(i * tile, tile)
        ids = lax.broadcasted_iota(jnp.int32, (tile, LANES), 1)
        logs = jnp.zeros((tile, LANES), F32)
        for h in range(heads):
            a0 = acc[h, pl.ds(at, tile), :]
            a1 = acc[h, pl.ds(pl.multiple_of(rows + at, tile), tile), :]
            t0, t1 = a0[:, VDIM:], a1[:, VDIM:]
            diff = a0[:, :VDIM] / t0 - lam_r[h] * (a1[:, :VDIM] / t1)
            out = (
                diff
                * lax.rsqrt(jnp.mean(diff * diff, axis=-1, keepdims=True) + EPS)
                * hgain_r[...].astype(F32)
            )
            both[pl.ds(at, tile), h * VDIM : (h + 1) * VDIM] = out.astype(BF)
            logs = jnp.where(ids == 2 * h, jnp.log(t0), logs)
            logs = jnp.where(ids == 2 * h + 1, jnp.log(t1), logs)
        log_r[pl.ds(at, tile), :] = logs[:, : 2 * heads]
        return carry

    lax.fori_loop(0, rows // tile, head_rows, 0)

    sq_copy.wait()
    inv = lax.rsqrt((sq_own[:, :1] + sq_in[:, :1]) / conv_total + EPS)
    cgain = cgain_r[:, pl.ds(pl.multiple_of(t * chans, LANES), chans)].astype(F32)
    both[:, att_rows:] = jax.nn.silu(conv[...] * inv * cgain).astype(BF)

    def pcopy(o):
        return pltpu.make_async_remote_copy(
            part_out.at[o], part_in.at[o], ps.at[o], pr.at[o], device_id=mate, device_id_type=MESH
        )

    ocols = gc.shape[2]
    mine = pl.ds(pl.multiple_of(t * half, half), half)
    other = pl.ds(pl.multiple_of((1 - t) * half, half), half)

    def out_block(o, _):
        part_out[o] = jnp.dot(both[other, :], gc[o], preferred_element_type=F32).astype(BF)
        pcopy(o).start()
        own = jnp.dot(both[mine, :], gc[o], preferred_element_type=F32)
        keep[o] = own

    out_block(s, None)
    for k in range(1, n):
        stage3(2, k)
        sides(k, out_block)

    def finish(o, carry):
        pcopy(o).wait_recv()
        pcopy(o).wait_send()
        mixed_r[:, pl.ds(pl.multiple_of(o * ocols, ocols), ocols)] = (
            keep[o] + part_in[o].astype(F32)
        ).astype(BF)
        return carry

    lax.fori_loop(0, n, finish, 0)

    for g in range(3):
        drain(g)

    @pl.when(has_right)
    def _():
        rim_copy.wait_send()
        for c in kvcopy(s):
            c.wait_send()

    for k in range(1, n):

        @pl.when((s >= k) & has_right)
        def _():
            for c in kvcopy(s - k):
                c.wait_send()


def body(n, conv_total, tokens, norm_gain, w_query, w_key, w_value, w_gv, w_gg, taps, cgain, hgain, lam, w_out):
    rows, width = tokens.shape
    heads = lam.shape[0]
    chans = w_gv.shape[1]
    qcols = w_query.shape[1]
    wrows = w_query.shape[0]
    ocols = w_out.shape[1]
    half = rows // 2
    any_ = pl.BlockSpec(memory_space=pl.ANY)
    vm = pl.BlockSpec(memory_space=pltpu.VMEM)
    sm = pl.BlockSpec(memory_space=pltpu.SMEM)
    dma = pltpu.SemaphoreType.DMA
    v = pltpu.VMEM
    return pl.pallas_call(
        functools.partial(kernel, n, conv_total),
        out_shape=(
            jax.ShapeDtypeStruct((half, width), BF),
            jax.ShapeDtypeStruct((rows, 2 * heads), F32),
        ),
        in_specs=[any_, vm, any_, any_, any_, any_, any_, vm, vm, vm, sm, any_],
        out_specs=(vm, vm),
        scratch_shapes=[
            v((rows, width), BF),
            v((rows, width), BF),
            v((n, wrows, qcols + 2 * LANES), BF),
            v((n, wrows, 2 * chans), BF),
            v((n, heads * VDIM + chans, ocols), BF),
            v((heads, 2 * rows, LANES), BF),
            v((n, rows, LANES), BF),
            v((n, rows, LANES), BF),
            v((heads, 2 * rows, 2 * VDIM), F32),
            v((rows, chans), BF),
            v((RIM, chans), BF),
            v((rows + RIM, chans), F32),
            v((rows, chans), F32),
            v((rows, LANES), F32),
            v((rows, LANES), F32),
            v((rows, heads * VDIM + chans), BF),
            v((n, half, ocols), BF),
            v((n, half, ocols), BF),
            v((n, half, ocols), F32),
            dma((8,)),
            dma((3, 2, n)),
            dma((3, n)),
            dma((3, n)),
            dma((3, n)),
            dma((3, n)),
            dma((3, n)),
            dma((3, n)),
            dma((3, n)),
            dma((3, n)),
            dma((3, n)),
            dma((2, n)),
            dma((2, n)),
            dma((2,)),
            dma((2,)),
            dma((n,)),
            dma((n,)),
        ],
        compiler_params=pltpu.CompilerParams(
            collective_id=0, has_side_effects=True, vmem_limit_bytes=60 * 1024 * 1024
        ),
    )(
        tokens,
        norm_gain.reshape(1, -1),
        w_query,
        w_key,
        w_value,
        w_gv,
        w_gg,
        taps,
        cgain.reshape(1, -1),
        hgain.reshape(1, -1),
        lam,
        w_out,
    )


def solution(mesh):
    n = mesh.shape["sp"]

    def run(*args):
        return body(n, args[8].shape[0], *args)

    return jax.shard_map(
        run,
        mesh=mesh,
        in_specs=(
            P(("fs", "sp"), None),
            P(),
            P("sp", "tp"),
            P("sp", "tp"),
            P("sp", "tp"),
            P("sp", "tp"),
            P("sp", "tp"),
            P(None, "tp"),
            P(),
            P(),
            P("tp"),
            P(None, "sp"),
        ),
        out_specs=(P(("fs", "sp", "tp"), None), P(("fs", "sp"), "tp")),
        check_vma=False,
    )
```

time: 279 us -> 104 us (0.37)
  the two profiles are of different devices: /device:TPU:25 before, /device:TPU:0 now
where the time goes in v1:
time: 104 us
  Pallas kernels  96.9 us (93%)
  local copies, waits for them, and re-layouts  6.53 us (6%)
    pallas_call x1, Pallas kernels, body(): pl.pallas_call(functools.partial(kernel, n, conv_total), out_shape=(jax.S...  96.9 us
    unnamed x1, local copies, waits for them, and re-layouts  2.3 us

profile of v1, /device:TPU:0, one launch (start us, length us, event | category | flops | bytes accessed | tf_op | source)
XLA Modules:
  0.0 104.1 jit_solution(7396023968017026908)
XLA Ops:
  0.6 1.3 %reshape.14.cgain_r = bf16[1,1024]{1,0:T(2,128)(2,1)} reshape(bf16[1024]{0:T(1024)(128)(2,1)} %param.20) | data formatting | bytes 4096 | tf_op jit(solution)/shard_map/reshape | solution.py:582
  1.9 1.3 %reshape.13.gain_r = bf16[1,2048]{1,0:T(2,128)(2,1)} reshape(bf16[2048]{0:T(1024)(128)(2,1)} %param.13) | data formatting | bytes 8192 | tf_op jit(solution)/shard_map/reshape | solution.py:575
  3.2 96.9 %shard_map.131 = (bf16[256,2048]{1,0:T(8,128)(2,1)}, f32[512,8]{1,0:T(8,128)}) custom-call(bf16[512,2048]{1,0:T(8,128)(2,1)} %tok_h.1, bf16[1,2048]{1,0:T(2,128)(2,1)} %reshape.13.gain_r, bf16[512,512]{1,0:T(8,128)(2,1)} %wq_h.1, bf16[512,128]{1,0:T(8,128)(2,1)} %wk_h.1, bf16[512,128]{1,0:T(8,128)(2,1)} %wv_h.1, bf16[512,512]{1,0:T(8,128)(2,1)} %wgv_h.1, ...), custom_call_target="tpu_custom_call" | custom-call | tf_op jit(solution)/shard_map/pallas_call | solution.py:524
  100.1 1.7 %copy.14 = f32[512,8]{0,1:T(8,128)} copy(f32[512,8]{1,0:T(8,128)} %get-tuple-element.3) | data formatting | bytes 32768 | tf_op jit(solution)/shard_map/pallas_call | solution.py:524
  101.8 2.3 %copy.16 = bf16[256,2048]{1,0:T(8,128)(2,1)} copy(bf16[256,2048]{1,0:T(8,128)(2,1)} %get-tuple-element.6) | data formatting | bytes 2097152

commit v2 on v1

--- a/solution.py
+++ b/solution.py
@@ -37,7 +37,8 @@
     log_r,
     tok,
     normed,
-    ga,
+    gkv,
+    gq,
     gb,
     gc,
     q2,
@@ -87,16 +88,16 @@
     chans = gated.shape[1]
     qcols = wq_h.shape[1]
     half = rows // 2
-    groups = (ga, gb, gc)
+    groups = (gkv, gq, gb, gc)
     has_left = s > 0
     has_right = s < n - 1
 
     d_rows = wq_h.shape[0]
     att_rows = heads * VDIM
     locals_ = [
-        (wq_h, ga.at[s, :, pl.ds(0, qcols)]),
-        (wk_h, ga.at[s, :, pl.ds(qcols, LANES)]),
-        (wv_h, ga.at[s, :, pl.ds(qcols + LANES, LANES)]),
+        (wk_h, gkv.at[s, :, pl.ds(0, LANES)]),
+        (wv_h, gkv.at[s, :, pl.ds(LANES, LANES)]),
+        (wq_h, gq.at[s]),
         (tok_h, tok),
         (wgv_h, gb.at[s, :, pl.ds(0, chans)]),
         (wgg_h, gb.at[s, :, pl.ds(chans, chans)]),
@@ -293,40 +294,59 @@
         def _():
             attend(s - k, False)
 
-    for c in copies[:3]:
+    items = [(g, k) for g in range(4) for k in range(1, n)]
+    per = n - 1
+    state = {"at": 0}
+
+    def advance(to):
+        to = min(to, len(items))
+        for i in range(state["at"], to):
+            stage1(*items[i])
+            if i == per:
+                own_send(2)
+            if i == 2 * per:
+                own_send(3)
+            if i > 0:
+                stage2(*items[i - 1])
+        state["at"] = max(state["at"], to)
+
+    def arrived(g):
+        for k in range(1, n):
+            stage3(g, k)
+
+    for c in copies[:2]:
         c.wait()
     own_send(0)
+    copies[2].wait()
+    own_send(1)
     copies[3].wait()
+
+    gain = gain_r[...].reshape(1, width).astype(F32)
 
     def norm_step(i, carry):
         at = pl.ds(pl.multiple_of(i * 32, 32), 32)
         x = tok[at, :].astype(F32)
         r = lax.rsqrt(jnp.mean(x * x, axis=-1, keepdims=True) + EPS)
-        normed[at, :] = (x * r * gain_r[...].astype(F32)).astype(BF)
+        normed[at, :] = (x * r * gain).astype(BF)
         return carry
 
-    lax.fori_loop(0, rows // 32, norm_step, 0)
+    def norm_rows(lo, hi):
+        lax.fori_loop(lo, hi, norm_step, 0)
+
+    steps = rows // 32
+    norm_rows(0, steps // 2)
+    advance(1)
+    norm_rows(steps // 2, steps)
     for c in copies[4:]:
         c.wait()
-
-    for k in range(1, n):
-        stage1(0, k)
-        if k == 1:
-            own_send(1)
-        if k > 1:
-            stage2(0, k - 1)
-    if n > 1:
-        stage2(0, n - 1)
-        stage1(1, 1)
-        own_send(2)
-    for k in range(1, n):
-        stage3(0, k)
+    advance(per + 2)
+    arrived(0)
 
     lane = lax.broadcasted_iota(jnp.int32, (rows, LANES), 1)
 
     kv = jnp.dot(
         normed[...],
-        ga[:, :, qcols : qcols + 2 * LANES].reshape(width, 2 * LANES),
+        gkv[...].reshape(width, 2 * LANES),
         preferred_element_type=F32,
     ).astype(BF)
     kbuf[s] = kv[:, :LANES]
@@ -337,9 +357,12 @@
         for c in kvcopy(s):
             c.start()
 
+    advance(2 * per + 2)
+    arrived(1)
+
     def q_step(h, carry):
         cols = pl.ds(pl.multiple_of(h * 2 * LANES, 2 * LANES), 2 * LANES)
-        q = jnp.dot(normed[...], ga[:, :, cols].reshape(width, 2 * LANES), preferred_element_type=F32)
+        q = jnp.dot(normed[...], gq[:, :, cols].reshape(width, 2 * LANES), preferred_element_type=F32)
         for e in range(2):
             one = q[:, e * LANES : (e + 1) * LANES]
             q2[2 * h + e, :rows, :] = jnp.where(lane < QK, one, 0.0).astype(BF)
@@ -348,23 +371,12 @@
 
     lax.fori_loop(0, heads // 2, q_step, 0)
 
-    if n > 2:
-        stage1(1, 2)
-    if n > 1:
-        stage2(1, 1)
     attend(s, True)
-    for k in range(3, n):
-        stage1(1, k)
-        stage2(1, k - 1)
-    if n > 1:
-        kv_take(1)
-    if n > 2:
-        stage2(1, n - 1)
-    if n > 1:
-        attend_back(1)
-        stage1(2, 1)
-    for k in range(1, n):
-        stage3(1, k)
+    advance(3 * per + 1)
+    kv_take(1)
+    attend_back(1)
+    advance(3 * per + 2)
+    arrived(2)
 
     def glu_step(i, carry):
         at = pl.multiple_of(i * 2 * LANES, 2 * LANES)
@@ -394,13 +406,10 @@
     def _():
         rim_copy.start()
 
-    for k in range(2, n):
-        stage1(2, k)
-        stage2(2, k - 1)
-        kv_take(k)
-        attend_back(k)
-    if n > 1:
-        stage2(2, n - 1)
+    if n > 2:
+        kv_take(2)
+        attend_back(2)
+    advance(len(items))
 
     @pl.when(has_left)
     def _():
@@ -433,6 +442,10 @@
         sq_own, sq_in, sqs.at[0], sqs.at[1], device_id=mate, device_id_type=MESH
     )
     sq_copy.start()
+
+    for k in range(3, n):
+        kv_take(k)
+        attend_back(k)
 
     def head_rows(i, carry):
         at = pl.multiple_of(i * tile, tile)
@@ -451,14 +464,15 @@
             both[pl.ds(at, tile), h * VDIM : (h + 1) * VDIM] = out.astype(BF)
             logs = jnp.where(ids == 2 * h, jnp.log(t0), logs)
             logs = jnp.where(ids == 2 * h + 1, jnp.log(t1), logs)
-        log_r[pl.ds(at, tile), :] = logs[:, : 2 * heads]
+        log_r[:, pl.ds(at, tile)] = logs.T[: 2 * heads, :]
         return carry
 
     lax.fori_loop(0, rows // tile, head_rows, 0)
+    stage2(*items[-1])
 
     sq_copy.wait()
     inv = lax.rsqrt((sq_own[:, :1] + sq_in[:, :1]) / conv_total + EPS)
-    cgain = cgain_r[:, pl.ds(pl.multiple_of(t * chans, LANES), chans)].astype(F32)
+    cgain = cgain_r[pl.ds(pl.multiple_of(t * chans, LANES), chans)].reshape(1, chans).astype(F32)
     both[:, att_rows:] = jax.nn.silu(conv[...] * inv * cgain).astype(BF)
 
     def pcopy(o):
@@ -478,7 +492,7 @@
 
     out_block(s, None)
     for k in range(1, n):
-        stage3(2, k)
+        stage3(3, k)
         sides(k, out_block)
 
     def finish(o, carry):
@@ -491,7 +505,7 @@
 
     lax.fori_loop(0, n, finish, 0)
 
-    for g in range(3):
+    for g in range(4):
         drain(g)
 
     @pl.when(has_right)
@@ -521,18 +535,19 @@
     sm = pl.BlockSpec(memory_space=pltpu.SMEM)
     dma = pltpu.SemaphoreType.DMA
     v = pltpu.VMEM
-    return pl.pallas_call(
+    mixed, logs = pl.pallas_call(
         functools.partial(kernel, n, conv_total),
         out_shape=(
             jax.ShapeDtypeStruct((half, width), BF),
-            jax.ShapeDtypeStruct((rows, 2 * heads), F32),
+            jax.ShapeDtypeStruct((2 * heads, rows), F32),
         ),
         in_specs=[any_, vm, any_, any_, any_, any_, any_, vm, vm, vm, sm, any_],
         out_specs=(vm, vm),
         scratch_shapes=[
             v((rows, width), BF),
             v((rows, width), BF),
-            v((n, wrows, qcols + 2 * LANES), BF),
+            v((n, wrows, 2 * LANES), BF),
+            v((n, wrows, qcols), BF),
             v((n, wrows, 2 * chans), BF),
             v((n, heads * VDIM + chans, ocols), BF),
             v((heads, 2 * rows, LANES), BF),
@@ -550,16 +565,16 @@
             v((n, half, ocols), BF),
             v((n, half, ocols), F32),
             dma((8,)),
-            dma((3, 2, n)),
-            dma((3, n)),
-            dma((3, n)),
-            dma((3, n)),
-            dma((3, n)),
-            dma((3, n)),
-            dma((3, n)),
-            dma((3, n)),
-            dma((3, n)),
-            dma((3, n)),
+            dma((4, 2, n)),
+            dma((4, n)),
+            dma((4, n)),
+            dma((4, n)),
+            dma((4, n)),
+            dma((4, n)),
+            dma((4, n)),
+            dma((4, n)),
+            dma((4, n)),
+            dma((4, n)),
             dma((2, n)),
             dma((2, n)),
             dma((2,)),
@@ -572,18 +587,19 @@
         ),
     )(
         tokens,
-        norm_gain.reshape(1, -1),
+        norm_gain,
         w_query,
         w_key,
         w_value,
         w_gv,
         w_gg,
         taps,
-        cgain.reshape(1, -1),
+        cgain,
         hgain.reshape(1, -1),
         lam,
         w_out,
     )
+    return mixed, logs.T
 
 
 def solution(mesh):

time: 104 us -> 98.2 us (0.944)
  the two profiles are of different devices: /device:TPU:0 before, /device:TPU:25 now
where the time goes in v2:
time: 98.2 us; the launch traced here: 98 us
  Pallas kernels  94.4 us (96%)
  local copies, waits for them, and re-layouts  2.92 us (3%)
    pallas_call x1, Pallas kernels, body(): pl.pallas_call(functools.partial(kernel, n, conv_total), out_shape=(jax.S...  94.4 us
    unnamed x4, local copies, waits for them, and re-layouts  2.92 us

profile of v2, /device:TPU:25, one launch (start us, length us, event | category | flops | bytes accessed | tf_op | source)
XLA Modules:
  0.0 98.0 jit_solution(8298501568618422372)
XLA Ops:
  0.6 94.4 %shard_map.131 = (bf16[256,2048]{1,0:T(8,128)(2,1)}, f32[8,512]{1,0:T(8,128)}) custom-call(bf16[512,2048]{1,0:T(8,128)(2,1)} %tok_h.1, bf16[2048]{0:T(1024)(128)(2,1)} %gain_r.1, bf16[512,512]{1,0:T(8,128)(2,1)} %wq_h.1, bf16[512,128]{1,0:T(8,128)(2,1)} %wk_h.1, bf16[512,128]{1,0:T(8,128)(2,1)} %wv_h.1, bf16[512,512]{1,0:T(8,128)(2,1)} %wgv_h.1, ...), custom_call_target="tpu_custom_call" | custom-call | tf_op jit(solution)/shard_map/pallas_call | solution.py:538
  95.0 0.0 copy-start
  95.1 2.3 %copy.16 = bf16[256,2048]{1,0:T(8,128)(2,1)} copy(bf16[256,2048]{1,0:T(8,128)(2,1)} %get-tuple-element.8) | data formatting | bytes 2097152
  97.4 0.0 copy-done
  97.4 0.6 copy.17
Async XLA Ops:
  95.0 2.3 %copy-start = (f32[8,512]{1,0:T(8,128)S(1)}, f32[8,512]{1,0:T(8,128)}, u32[]{:S(2)}) copy-start(f32[8,512]{1,0:T(8,128)} %get-tuple-element.5) | copy-start | bytes 49156

commit v3 on v2

--- a/solution.py
+++ b/solution.py
@@ -188,15 +188,20 @@
         def _():
             zcopy(g, s, False).start()
 
-    def stage1(g, k):
+    def stage0(g, k):
         def go(o, right_way):
             zcopy(g, o, right_way).wait_recv()
-            xcopy(g, o, f).start()
-            ycopy(g, o, f).start()
 
             @pl.when(has_right if right_way else has_left)
             def _():
                 zcopy(g, o, right_way).start()
+
+        sides(k, go)
+
+    def stage1(g, k):
+        def go(o, right_way):
+            xcopy(g, o, f).start()
+            ycopy(g, o, f).start()
 
         sides(k, go)
 
@@ -296,11 +301,14 @@
 
     items = [(g, k) for g in range(4) for k in range(1, n)]
     per = n - 1
-    state = {"at": 0}
+    state = {"at": 0, "in": 0}
 
     def advance(to):
         to = min(to, len(items))
         for i in range(state["at"], to):
+            if state["in"] == i:
+                stage0(*items[i])
+                state["in"] += 1
             stage1(*items[i])
             if i == per:
                 own_send(2)
@@ -308,6 +316,9 @@
                 own_send(3)
             if i > 0:
                 stage2(*items[i - 1])
+            if i >= 2 * per and i + 1 < len(items):
+                stage0(*items[i + 1])
+                state["in"] += 1
         state["at"] = max(state["at"], to)
 
     def arrived(g):

time: 98.2 us -> 104 us (1.059)
  Pallas kernels: 94.4 us -> 99.9 us
    pallas_call x1, Pallas kernels: 94.4 us -> 99.9 us  [body(): pl.pallas_call(functools.partial(kernel, n, conv_total), out_shape=(jax.S...]
where the time goes in v3:
time: 104 us; the launch traced here: 103 us
  Pallas kernels  99.9 us (96%)
  local copies, waits for them, and re-layouts  2.92 us (3%)
    pallas_call x1, Pallas kernels, body(): pl.pallas_call(functools.partial(kernel, n, conv_total), out_shape=(jax.S...  99.9 us
    unnamed x4, local copies, waits for them, and re-layouts  2.92 us

profile of v3, /device:TPU:25, one launch (start us, length us, event | category | flops | bytes accessed | tf_op | source)
XLA Modules:
  0.0 103.5 jit_solution(10528002152476044307)
XLA Ops:
  0.6 99.9 %shard_map.131 = (bf16[256,2048]{1,0:T(8,128)(2,1)}, f32[8,512]{1,0:T(8,128)}) custom-call(bf16[512,2048]{1,0:T(8,128)(2,1)} %tok_h.1, bf16[2048]{0:T(1024)(128)(2,1)} %gain_r.1, bf16[512,512]{1,0:T(8,128)(2,1)} %wq_h.1, bf16[512,128]{1,0:T(8,128)(2,1)} %wk_h.1, bf16[512,128]{1,0:T(8,128)(2,1)} %wv_h.1, bf16[512,512]{1,0:T(8,128)(2,1)} %wgv_h.1, ...), custom_call_target="tpu_custom_call" | custom-call | tf_op jit(solution)/shard_map/pallas_call | solution.py:549
  100.6 0.0 copy-start
  100.6 2.3 %copy.16 = bf16[256,2048]{1,0:T(8,128)(2,1)} copy(bf16[256,2048]{1,0:T(8,128)(2,1)} %get-tuple-element.8) | data formatting | bytes 2097152
  102.9 0.0 copy-done
  102.9 0.6 copy.17
Async XLA Ops:
  100.6 2.3 %copy-start = (f32[8,512]{1,0:T(8,128)S(1)}, f32[8,512]{1,0:T(8,128)}, u32[]{:S(2)}) copy-start(f32[8,512]{1,0:T(8,128)} %get-tuple-element.5) | copy-start | bytes 49156
